TPU v7x, 512 devices: a 8x2x16 block of a 8x8x16 slice. The times are simulated.
512 devices in a mesh: grp: 2 (over y), sp: 32 (over z, core), tp: 8 (over x).
Axes of the slice: x: 8, y: 2, z: 16, core: 2. Of those that a mesh axis runs over, the one named last changes fastest.
The devices are a block of a 8x8x16 slice.
Arguments:
- residual: bfloat16 [16384, 2048], P(('grp', 'sp')), parts along dimension 0, may hold values from -34 to 34
- queries: bfloat16 [16384, 1024], P(('grp', 'sp'), 'tp'), parts along dimension 0, may hold values from -400 to 400
- keys: bfloat16 [16384, 512], P(('grp', 'sp'), 'tp'), parts along dimension 0, may hold values from -8 to 8
- values: bfloat16 [16384, 512], P(('grp', 'sp'), 'tp'), parts along dimension 0, may hold values from -6 to 6
- segments: int32 [16384], P(('grp', 'sp')), parts along dimension 0, may hold values from 0 to 16, never falling along the last dimension, each value on 1 to 768 neighbouring positions
- routes: int32 [16384, 2], P(('grp', 'sp')), parts along dimension 0, may hold values from 0 to 31, all different within a row; in each aligned block of 256 rows (0 to 255, 256 to 511, ...) at most 32 rows name the same one
- route_weight: float32 [16384, 2], P(('grp', 'sp')), parts along dimension 0, may hold values from 0.3 to 3
- sinks: float32 [16], P('tp'), may hold values from 1 to 6
- out_weight: bfloat16 [1024, 2048], P('tp'), may hold values from -1 to 1
- norm_gain: float32 [2048], replicated, may hold values from 0.1 to 1.9
- expert_gate: bfloat16 [32, 2048, 1024], P('sp', None, 'tp'), may hold values from -0.125 to 0.125
- expert_up: bfloat16 [32, 2048, 1024], P('sp', None, 'tp'), may hold values from -0.125 to 0.125
- expert_down: bfloat16 [32, 1024, 2048], P('sp', None, 'tp'), may hold values from -0.1875 to 0.1875
- shared_gate: bfloat16 [2048, 1024], P(None, 'tp'), may hold values from -0.125 to 0.125
- shared_up: bfloat16 [2048, 1024], P(None, 'tp'), may hold values from -0.125 to 0.125
- shared_down: bfloat16 [1024, 2048], P(None, 'tp'), may hold values from -0.1875 to 0.1875
Outputs:
- mixed: bfloat16 [16384, 2048], P(('grp', 'sp'), 'tp'), parts along dimension 0
There are 2 independent parts, one for each index of `grp`. A program takes and returns all parts, laid end to end along the dimension named above; an argument that names none is the same for every part. Nothing has to cross between parts.
Inputs may be any that keep to these rules, and one draw needn't show every extreme that they name: `routes`: each row names 2 different experts. In the rows of one device no expert is named by more than 32 rows, and in some device's rows an expert is named by exactly 32. `segments`: document numbers never fall along the positions; every document spans 1 to 768 positions and one spans exactly 768.
All inputs are finite; a program needn't handle non-finite values.
Results may differ from a plain program's by a relative error of at most 0.0065.
Values may be sent and summed in bfloat16 or wider, within the bound.
A program may use at most 64 MiB of HBM per device.

v0:
```python
import jax
import jax.numpy as jnp
from jax import lax
from jax.sharding import Mesh
from jax.sharding import PartitionSpec as P

HEAD_DIM = 64
WINDOW = 128
SP = ("sp_0", "sp_1")
GRP_SP = ("grp", "sp_0", "sp_1")
epsilon = 1e-06


def passed_along(value, axis, steps):
    count = lax.axis_size(axis)
    leading, last = (max(0, -steps), min(count, count - steps))
    return lax.ppermute(value, axis, [(source, source + steps) for source in range(leading, last)])


def split_up(array, dim, size):
    shape = array.shape
    blocks = array.reshape(*shape[:dim], size, shape[dim] // size, *shape[dim + 1 :])
    return jnp.moveaxis(blocks, dim, 0)


def sent_and_summed(array, axis, dim):
    size = lax.axis_size(axis)
    blocks = lax.all_to_all(split_up(array, dim, size), axis, 0, 0, tiled=True)
    return jnp.sum(blocks.astype(jnp.float32), axis=0)


def sent_to_all(array, axis):
    size = lax.axis_size(axis)
    return lax.all_to_all(
        jnp.broadcast_to(array[None], (size, *array.shape)), axis, 0, 0, tiled=True
    )


def in_order(blocks, dim):
    blocks = jnp.moveaxis(blocks, 0, dim)
    shape = blocks.shape
    return blocks.reshape(*shape[:dim], shape[dim] * shape[dim + 1], *shape[dim + 2 :])


def collect(array, axis, dim):
    blocks = sent_to_all(array, axis)
    return in_order(blocks, dim)


def moved_by_axis(blocks, axes, order):
    shape = [lax.axis_size(a) for a in axes]
    blocks = blocks.reshape(*shape, *blocks.shape[1:])
    for k in order:
        blocks = lax.all_to_all(blocks, axes[k], split_axis=k, concat_axis=k, tiled=True)
    return blocks.reshape(-1, *blocks.shape[len(axes) :])


def two_step_exchange(array, groups, order, split_dim, concat_dim):
    size = lax.axis_size(groups[0]) * lax.axis_size(groups[1])
    blocks = split_up(array, split_dim, size)
    return in_order(moved_by_axis(blocks, groups, order), concat_dim)


def sent_together(arrays, axis, dim, along):
    ends, at = ([], 0)
    for a in arrays[:-1]:
        at += a.shape[along]
        ends.append(at)
    both = jnp.concatenate(arrays, axis=along)
    return tuple(jnp.split(lax.all_gather(both, axis, axis=dim, tiled=True), ends, axis=along))


def banded(prev_rows, own_rows, window_len):
    blocks = own_rows.shape[0] // window_len
    joined = jnp.concatenate([prev_rows, own_rows], axis=0)
    shaped = joined.reshape((blocks + 1, window_len) + own_rows.shape[1:])
    return jnp.concatenate([shaped[:-1], shaped[1:]], axis=1)


def shards(
    residual,
    queries,
    keys,
    values,
    segments,
    routes,
    route_weight,
    sinks,
    out_weight,
    norm_gain,
    expert_gate,
    expert_up,
    expert_down,
    shared_gate,
    shared_up,
    shared_down,
):
    rows_here = residual.shape[0]
    model_width = residual.shape[1]
    tp_count = lax.axis_size("tp")
    tp_index = lax.axis_index("tp")
    head_local = queries.shape[1] // HEAD_DIM
    kv_local = keys.shape[1] // HEAD_DIM
    group_size = head_local // kv_local
    window_len = WINDOW
    blocks = rows_here // window_len
    own_marks = (segments % 256 + 1).astype(jnp.bfloat16)
    prev_keys, prev_values, prev_marks = passed_along(
        (
            keys[rows_here - window_len :],
            values[rows_here - window_len :],
            own_marks[rows_here - window_len :],
        ),
        SP,
        1,
    )
    key_band = banded(prev_keys, keys, window_len).reshape(
        blocks, 2 * window_len, kv_local, HEAD_DIM
    )
    value_band = banded(prev_values, values, window_len).reshape(
        blocks, 2 * window_len, kv_local, HEAD_DIM
    )
    mark_band = banded(prev_marks, own_marks, window_len).astype(jnp.float32)
    query_marks = own_marks.reshape(blocks, window_len).astype(jnp.float32)
    query_blocks = queries.reshape(blocks, window_len, kv_local, group_size, HEAD_DIM)
    scores = jnp.einsum(
        "nqhgd,nkhd->nhgqk", query_blocks, key_band, preferred_element_type=jnp.float32
    ) * HEAD_DIM ** (-0.5)
    offsets = jnp.arange(window_len)[:, None] + window_len - jnp.arange(2 * window_len)[None, :]
    allowed = (
        (offsets >= 0) & (offsets < window_len) & (query_marks[:, :, None] == mark_band[:, None, :])
    )
    sink_logits = sinks.reshape(kv_local, group_size)[None, :, :, None]
    masked = jnp.where(allowed[:, None, None], scores, -jnp.inf)
    top_score = jnp.maximum(jnp.max(masked, axis=-1), sink_logits)
    exp_terms = jnp.where(allowed[:, None, None], jnp.exp(scores - top_score[..., None]), 0.0)
    denominator = jnp.sum(exp_terms, axis=-1) + jnp.exp(sink_logits - top_score)
    probabilities = (exp_terms / denominator[..., None]).astype(jnp.bfloat16)
    attended = jnp.einsum(
        "nhgqk,nkhd->nqhgd", probabilities, value_band, preferred_element_type=jnp.float32
    )
    attended = attended.astype(jnp.bfloat16).reshape(rows_here, head_local * HEAD_DIM)
    partial_value = jnp.dot(attended, out_weight, preferred_element_type=jnp.float32)
    col_width = model_width // tp_count
    col_start = tp_index * col_width
    share_sum = sent_and_summed(partial_value.astype(jnp.bfloat16), "tp", 1)
    residual_cols = lax.dynamic_slice_in_dim(residual, col_start, col_width, 1)
    updated_cols = (residual_cols.astype(jnp.float32) + share_sum).astype(jnp.bfloat16)
    cols_f32 = updated_cols.astype(jnp.float32)
    squares = lax.psum(jnp.sum(cols_f32 * cols_f32, axis=-1), "tp")
    inv_rms = lax.rsqrt(squares / model_width + epsilon)
    gain_cols = lax.dynamic_slice_in_dim(norm_gain, col_start, col_width, 0)
    normed_cols = (cols_f32 * inv_rms[:, None] * gain_cols).astype(jnp.bfloat16)
    normed = collect(normed_cols, "tp", 1)
    shared_pre = jnp.dot(normed, shared_gate, preferred_element_type=jnp.float32)
    shared_lin = jnp.dot(normed, shared_up, preferred_element_type=jnp.float32)
    shared_act = (jax.nn.silu(shared_pre) * shared_lin).astype(jnp.bfloat16)
    top_count = routes.shape[1]
    experts = lax.axis_size(SP)
    capacity = 2 * rows_here * top_count // experts
    flat_ids = routes.reshape(-1)
    one_hot = (flat_ids[:, None] == jnp.arange(experts, dtype=jnp.int32)[None, :]).astype(jnp.int32)
    rank_in = jnp.cumsum(one_hot, axis=0) - one_hot
    slot_dest = flat_ids * capacity + jnp.sum(rank_in * one_hot, axis=1)
    token_of = jnp.arange(rows_here * top_count, dtype=jnp.int32) // top_count
    slot_token = jnp.full((experts * capacity,), -1, jnp.int32).at[slot_dest].set(token_of)
    filled = slot_token >= 0
    safe_token = jnp.where(filled, slot_token, 0)
    outgoing = jnp.where(filled[:, None], normed_cols[safe_token], jnp.zeros((), jnp.bfloat16))
    pieces = two_step_exchange(
        outgoing.reshape(experts, capacity, col_width), ("sp_0", "sp_1"), (1, 0), 0, 0
    )
    arrived = lax.all_gather(pieces, "tp", axis=2, tiled=True)
    expert_rows = arrived.reshape(-1, model_width)
    gate_pre = jnp.dot(expert_rows, expert_gate[0], preferred_element_type=jnp.float32)
    up_lin = jnp.dot(expert_rows, expert_up[0], preferred_element_type=jnp.float32)
    expert_act = (jax.nn.silu(gate_pre) * up_lin).astype(jnp.bfloat16)
    gathered_expert, gathered_shared = sent_together((expert_act, shared_act), "tp", 1, 0)
    expert_out = jnp.dot(
        gathered_expert, expert_down[0], preferred_element_type=jnp.float32
    ).astype(jnp.bfloat16)
    returned = lax.all_to_all(
        expert_out.reshape(experts, capacity, col_width),
        SP,
        split_axis=0,
        concat_axis=0,
        tiled=True,
    )
    returned = returned.reshape(experts * capacity, col_width)
    picked = returned[slot_dest].astype(jnp.float32).reshape(rows_here, top_count, col_width)
    routed = jnp.sum(picked * route_weight[:, :, None], axis=1)
    shared_cols = jnp.dot(gathered_shared, shared_down, preferred_element_type=jnp.float32)
    return (updated_cols.astype(jnp.float32) + shared_cols + routed).astype(jnp.bfloat16)


def solution(mesh):
    torus = Mesh(
        mesh.devices.reshape(mesh.shape["grp"], 16, 2, mesh.shape["tp"]),
        ("grp", "sp_0", "sp_1", "tp"),
    )
    in_specs = (
        P(GRP_SP, None),
        P(GRP_SP, "tp"),
        P(GRP_SP, "tp"),
        P(GRP_SP, "tp"),
        P(GRP_SP),
        P(GRP_SP, None),
        P(GRP_SP, None),
        P("tp"),
        P("tp", None),
        P(),
        P(SP, None, "tp"),
        P(SP, None, "tp"),
        P(SP, None, "tp"),
        P(None, "tp"),
        P(None, "tp"),
        P(None, "tp"),
    )
    out_specs = P(GRP_SP, "tp")
    return jax.shard_map(
        shards, mesh=torus, in_specs=in_specs, out_specs=out_specs, check_vma=False
    )
```

profile of v0, /device:TPU:65, one launch (start us, length us, event | category | flops | bytes accessed | tf_op | source)
XLA Modules:
  0.0 356.7 jit_solution(9728244078039882902)
XLA Ops:
  7.3 7.1 %collective-permute-start.1 = (bf16[128]{0:T(256)(128)(2,1)S(1)}, bf16[128]{0:T(256)(128)(2,1)S(1)}, u32[]{:S(2)}, u32[]{:S(2)}) collective-permute-start(bf16[128]{0:T(256)(128)(2,1)S(1)} %slice.57), channel_id=1, source_target_pairs={{0,8},{8,16},{16,24},{24,32},{32,40},{40,48},{48,56},{56,64},{64,7... | collective-permute-start | bytes 776 | tf_op jit(solution)/shard_map/ppermute | solution.py:17
  15.1 1.9 collective-permute-start.2
  17.8 6.1 %collective-permute-start = (bf16[128,64]{0,1:T(8,128)(2,1)S(1)}, bf16[128,64]{0,1:T(8,128)(2,1)S(1)}, u32[]{:S(2)}, u32[]{:S(2)}) collective-permute-start(bf16[128,64]{0,1:T(8,128)(2,1)S(1)} %slice.53), channel_id=1, source_target_pairs={{0,8},{8,16},{16,24},{24,32},{32,40},{40,48},{48,56},{56,64},{64,7... | collective-permute-start | bytes 49160 | tf_op jit(solution)/shard_map/ppermute | solution.py:17
  26.4 24.3 %collective-permute-done.1 = bf16[128]{0:T(256)(128)(2,1)S(1)} collective-permute-done((bf16[128]{0:T(256)(128)(2,1)S(1)}, bf16[128]{0:T(256)(128)(2,1)S(1)}, u32[]{:S(2)}, u32[]{:S(2)}) %collective-permute-start.1) | collective-permute-done | bytes 288 | tf_op jit(solution)/shard_map/ppermute | solution.py:17
  50.8 1.9 collective-permute-done.2
  56.9 1.1 copy.79
  57.9 3.8 %all-to-all-start = ((bf16[8,256,256]{2,1,0:T(8,128)(2,1)}), bf16[8,256,256]{2,1,0:T(8,128)(2,1)S(1)}, u32[]{:S(2)}, u32[]{:S(2)}) async-start(bf16[8,256,256]{2,1,0:T(8,128)(2,1)} %bitcast.106), calls=%async_computation | async-start | bytes 2097152 | tf_op jit(solution)/shard_map/all_to_all | solution.py:28
  62.5 1.2 reduce-window.6
  64.1 2.4 scatter_custom_fusion
  67.4 19.8 %all-to-all-done = bf16[8,256,256]{2,1,0:T(8,128)(2,1)S(1)} async-done(((bf16[8,256,256]{2,1,0:T(8,128)(2,1)}), bf16[8,256,256]{2,1,0:T(8,128)(2,1)S(1)}, u32[]{:S(2)}, u32[]{:S(2)}) %all-to-all-start) | async-done | bytes 1048608 | tf_op jit(solution)/shard_map/all_to_all | solution.py:28
  88.4 11.1 %psum.7 = f32[256]{0:T(256)S(1)} all-reduce(f32[256]{0:T(256)S(1)} %get-tuple-element.5), channel_id=1, replica_groups=mesh['grp'=2,'sp_0'=16,'sp_1'=2,'tp'=8] {'tp'}, use_global_device_ids=true, to_apply=%region_8.9 | all-reduce | flops 256 | bytes 2048 | tf_op jit(solution)/shard_map/psum | solution.py:150
  99.6 3.9 %gather_fusion = bf16[1024,256]{1,0:T(8,128)(2,1)S(1)} fusion(bf16[256,256]{1,0:T(8,128)(2,1)S(1)} %fusion.19, s32[1024]{0:T(1024)S(1)} %fusion.37), kind=kCustom, calls=%fused_computation | custom fusion | bytes 1052672 | tf_op jit(solution)/shard_map/gather | solution.py:169
  103.8 11.5 %all_to_all.25 = bf16[16,2,1,32,256]{4,3,0,2,1:T(8,128)(2,1)S(1)} all-to-all(bf16[16,2,1,32,256]{4,3,0,2,1:T(8,128)(2,1)S(1)} %copy_select_fusion), channel_id=1, replica_groups=mesh['grp'=2,'sp_0'=16,'sp_1'=2,'tp'=8] {'sp_1'}, dimensions={1} | all-to-all | bytes 1048576 | tf_op jit(solution)/shard_map/all_to_all | solution.py:54
  115.3 36.5 %all_to_all.26 = bf16[16,2,1,32,256]{4,3,1,2,0:T(8,128)(2,1)} all-to-all(bf16[16,2,1,32,256]{4,3,1,2,0:T(8,128)(2,1)S(1)} %copy.49), channel_id=1, replica_groups=mesh['grp'=2,'sp_0'=16,'sp_1'=2,'tp'=8] {'sp_0'}, dimensions={0} | all-to-all | bytes 1048576 | tf_op jit(solution)/shard_map/all_to_all | solution.py:54
  152.2 24.5 %all_to_all.27 = bf16[8,256,256]{1,2,0:T(8,128)(2,1)S(1)} all-to-all(bf16[8,256,256]{1,2,0:T(8,128)(2,1)S(1)} %broadcast_in_dim.70), channel_id=1, replica_groups=mesh['grp'=2,'sp_0'=16,'sp_1'=2,'tp'=8] {'tp'}, dimensions={0} | all-to-all | bytes 2097152 | tf_op jit(solution)/shard_map/all_to_all | solution.py:34
  177.6 47.7 %all-gather.3.cloned.1.call-done = bf16[32,32,2048]{2,1,0:T(8,128)(2,1)} async-done(((bf16[32,32,256]{2,1,0:T(8,128)(2,1)}), bf16[32,32,2048]{2,1,0:T(8,128)(2,1)}) %all-gather.3.cloned.1.call-update) | async-done | bytes 4194320 | tf_op jit(solution)/shard_map/all_gather | solution.py:173
  225.3 3.6 %fusion.14 = f32[1024,128]{1,0:T(8,128)S(1)} fusion(bf16[1024,2048]{1,0:T(8,128)(2,1)} %bitcast.108, bf16[1,2048,128]{2,1,0:T(8,128)(2,1)S(1)} %copy-done.2), kind=kOutput, calls=%fused_computation.23 | convolution fusion | flops 536870912 | bytes 5242880 | tf_op jit(solution)/shard_map/dot_general | solution.py:175
  229.0 1.2 fusion.6
  231.0 59.2 %all-gather.5.cloned.1.call-done = bf16[1280,1024]{1,0:T(8,128)(2,1)} async-done(((bf16[1280,128]{1,0:T(8,128)(2,1)}), bf16[1280,1024]{1,0:T(8,128)(2,1)}) %all-gather.5.cloned.1.call-update) | async-done | bytes 2621456 | tf_op jit(solution)/shard_map/all_gather | solution.py:70
  290.2 3.1 fusion.2
  293.3 18.3 %all-to-all-start.4 = ((bf16[32,32,256]{2,1,0:T(8,128)(2,1)}), bf16[32,32,256]{2,1,0:T(8,128)(2,1)S(1)}, u32[]{:S(2)}, u32[]{:S(2)}) async-start(bf16[32,32,256]{2,1,0:T(8,128)(2,1)} %bitcast.25), calls=%async_computation.4 | async-start | bytes 1048576 | tf_op jit(solution)/shard_map/all_to_all | solution.py:182
  311.8 33.1 %all-to-all-done.4 = bf16[32,32,256]{2,1,0:T(8,128)(2,1)S(1)} async-done(((bf16[32,32,256]{2,1,0:T(8,128)(2,1)}), bf16[32,32,256]{2,1,0:T(8,128)(2,1)S(1)}, u32[]{:S(2)}, u32[]{:S(2)}) %all-to-all-start.4) | async-done | bytes 524320 | tf_op jit(solution)/shard_map/all_to_all | solution.py:182
  344.9 1.9 gather_fusion.1
  347.9 2.0 fusion.8
  (80 shorter events, 15.7 us)
Async XLA Ops:
  6.5 49.8 %copy-start = (bf16[128,2048]{1,0:T(8,128)(2,1)S(1)}, bf16[128,2048]{1,0:T(8,128)(2,1)}, u32[]{:S(2)}) copy-start(bf16[128,2048]{1,0:T(8,128)(2,1)} %param.24) | copy-start | bytes 1572868
  7.3 43.4 %collective-permute-start.1 = (bf16[128]{0:T(256)(128)(2,1)S(1)}, bf16[128]{0:T(256)(128)(2,1)S(1)}, u32[]{:S(2)}, u32[]{:S(2)}) collective-permute-start(bf16[128]{0:T(256)(128)(2,1)S(1)} %slice.57), channel_id=1, source_target_pairs={{0,8},{8,16},{16,24},{24,32},{32,40},{40,48},{48,56},{56,64},{64,7... | collective-permute-start | bytes 776 | tf_op jit(solution)/shard_map/ppermute | solution.py:17
  15.1 37.6 %collective-permute-start.2 = (bf16[128,64]{0,1:T(8,128)(2,1)S(1)}, bf16[128,64]{0,1:T(8,128)(2,1)S(1)}, u32[]{:S(2)}, u32[]{:S(2)}) collective-permute-start(bf16[128,64]{0,1:T(8,128)(2,1)S(1)} %slice.60), channel_id=1, source_target_pairs={{0,8},{8,16},{16,24},{24,32},{32,40},{40,48},{48,56},{56,64},{64,7... | collective-permute-start | bytes 49160 | tf_op jit(solution)/shard_map/ppermute | solution.py:17
  17.8 37.6 %collective-permute-start = (bf16[128,64]{0,1:T(8,128)(2,1)S(1)}, bf16[128,64]{0,1:T(8,128)(2,1)S(1)}, u32[]{:S(2)}, u32[]{:S(2)}) collective-permute-start(bf16[128,64]{0,1:T(8,128)(2,1)S(1)} %slice.53), channel_id=1, source_target_pairs={{0,8},{8,16},{16,24},{24,32},{32,40},{40,48},{48,56},{56,64},{64,7... | collective-permute-start | bytes 49160 | tf_op jit(solution)/shard_map/ppermute | solution.py:17
  56.4 5.4 %copy-start.5 = (s32[256,2]{0,1:T(2,128)S(1)}, s32[256,2]{0,1:T(2,128)}, u32[]{:S(2)}) copy-start(s32[256,2]{0,1:T(2,128)} %param.21) | copy-start | bytes 6148
  57.9 29.3 %all-to-all-start = ((bf16[8,256,256]{2,1,0:T(8,128)(2,1)}), bf16[8,256,256]{2,1,0:T(8,128)(2,1)S(1)}, u32[]{:S(2)}, u32[]{:S(2)}) async-start(bf16[8,256,256]{2,1,0:T(8,128)(2,1)} %bitcast.106), calls=%async_computation | async-start | bytes 2097152 | tf_op jit(solution)/shard_map/all_to_all | solution.py:28
  61.7 163.6 %all-gather.3.cloned.1.call-start = ((), (), s32[]{:S(2)}) async-start(), calls=%async_computation.5 | async-start | bytes 4718592 | tf_op jit(solution)/shard_map/all_gather | solution.py:173
  115.3 61.3 %copy-start.4 = (bf16[2048,128]{1,0:T(8,128)(2,1)S(1)}, bf16[2048,128]{1,0:T(8,128)(2,1)}, u32[]{:S(2)}) copy-start(bf16[2048,128]{1,0:T(8,128)(2,1)} %param.29) | copy-start | bytes 1572868
  151.9 25.2 %copy-start.7 = (bf16[2048,128]{1,0:T(8,128)(2,1)S(1)}, bf16[2048,128]{1,0:T(8,128)(2,1)}, u32[]{:S(2)}) copy-start(bf16[2048,128]{1,0:T(8,128)(2,1)} %param.30) | copy-start | bytes 1572868
  151.9 138.3 %all-gather.5.cloned.1.call-start = ((), (), s32[]{:S(2)}) async-start(), calls=%async_computation.6 | async-start | bytes 2949120 | tf_op jit(solution)/shard_map/all_gather | solution.py:70
  152.1 73.2 %copy-start.2 = (bf16[1,2048,128]{2,1,0:T(8,128)(2,1)S(1)}, bf16[1,2048,128]{2,1,0:T(8,128)(2,1)}, u32[]{:S(2)}) copy-start(bf16[1,2048,128]{2,1,0:T(8,128)(2,1)} %param.26) | copy-start | bytes 1572868
  225.3 3.6 %copy-start.1 = (bf16[32,32,2048]{2,1,0:T(8,128)(2,1)S(1)}, bf16[32,32,2048]{2,1,0:T(8,128)(2,1)}, u32[]{:S(2)}) copy-start(bf16[32,32,2048]{2,1,0:T(8,128)(2,1)} %all-gather.3.cloned.1.call-done) | copy-start | bytes 12582916
  225.3 3.6 %copy-start.8 = (bf16[1,2048,128]{2,1,0:T(8,128)(2,1)S(1)}, bf16[1,2048,128]{2,1,0:T(8,128)(2,1)}, u32[]{:S(2)}) copy-start(bf16[1,2048,128]{2,1,0:T(8,128)(2,1)} %param.27) | copy-start | bytes 1572868
  229.0 61.2 %copy-start.9 = (bf16[1,1024,256]{2,1,0:T(8,128)(2,1)S(1)}, bf16[1,1024,256]{2,1,0:T(8,128)(2,1)}, u32[]{:S(2)}) copy-start(bf16[1,1024,256]{2,1,0:T(8,128)(2,1)} %param.28) | copy-start | bytes 1572868
  231.0 80.6 %copy-start.6 = (f32[256,2]{0,1:T(2,128)S(1)}, f32[256,2]{0,1:T(2,128)}, u32[]{:S(2)}) copy-start(f32[256,2]{0,1:T(2,128)} %param.22) | copy-start | bytes 6148
  293.3 54.6 %copy-start.3 = (bf16[1024,256]{1,0:T(8,128)(2,1)S(1)}, bf16[1024,256]{1,0:T(8,128)(2,1)}, u32[]{:S(2)}) copy-start(bf16[1024,256]{1,0:T(8,128)(2,1)} %param.31) | copy-start | bytes 1572868
  293.3 51.6 %all-to-all-start.4 = ((bf16[32,32,256]{2,1,0:T(8,128)(2,1)}), bf16[32,32,256]{2,1,0:T(8,128)(2,1)S(1)}, u32[]{:S(2)}, u32[]{:S(2)}) async-start(bf16[32,32,256]{2,1,0:T(8,128)(2,1)} %bitcast.25), calls=%async_computation.4 | async-start | bytes 1048576 | tf_op jit(solution)/shard_map/all_to_all | solution.py:182
Sparse Core Ops, SparseCore 0:
  152.0 73.2 all-gather.2
  231.1 59.0 all-gather.4
where the time goes:
time: 358 us; the launch traced here: 357 us
  waiting for transfers between devices  186 us (52%)
  blocking collectives  83.5 us (23%)
  starting transfers between devices  37.3 us (10%)
  local copies, waits for them, and re-layouts  15.8 us (4%)
  between operations  13.8 us (4%)
  matrix products  11.9 us (3%)
  other arithmetic  8.26 us (2%)
    all_gather x1, waiting for transfers between devices, sent_together(): lax.all_gather(both, axis, axis=dim, tiled=True)  59.2 us
    all_to_all x2, blocking collectives, moved_by_axis(): lax.all_to_all(blocks, axes[k], split_axis=k, concat_axis=k, tiled=True)  48 us
    all_gather x1, waiting for transfers between devices, shards(): arrived = lax.all_gather(pieces, 'tp', axis=2, tiled=True)  47.7 us
    all_to_all x1, waiting for transfers between devices, shards(): lax.all_to_all(expert_out.reshape(experts, capacity, col_width), SP, spli...  33.1 us
    ppermute x3, waiting for transfers between devices, passed_along(): lax.ppermute(value, axis, [(source, source + steps) for source in range(l...  26.1 us
    all_to_all x1, blocking collectives, sent_to_all(): lax.all_to_all(jnp.broadcast_to(array[None], (size, *array.shape)), axis,...  24.5 us
    all_to_all x1, waiting for transfers between devices, sent_and_summed(): blocks = lax.all_to_all(split_up(array, dim, size), axis, 0, 0, tiled=True)  19.8 us
    all_to_all x1, starting transfers between devices, shards(): lax.all_to_all(expert_out.reshape(experts, capacity, col_width), SP, spli...  18.3 us
  transfers between devices with their start and end apart: 7, of which 6 were waited for; matrix products, arithmetic and copies ran while one was open for 4% of the time, Pallas kernels for 0%

commit v1 on v0

--- a/solution.py
+++ b/solution.py
@@ -170,7 +170,10 @@
     pieces = two_step_exchange(
         outgoing.reshape(experts, capacity, col_width), ("sp_0", "sp_1"), (1, 0), 0, 0
     )
-    arrived = lax.all_gather(pieces, "tp", axis=2, tiled=True)
+    arrived = jnp.concatenate(
+        lax.all_to_all(jnp.stack(tuple((pieces for _ in range(lax.psum(1, "tp"))))), "tp", 0, 0),
+        axis=2,
+    )
     expert_rows = arrived.reshape(-1, model_width)
     gate_pre = jnp.dot(expert_rows, expert_gate[0], preferred_element_type=jnp.float32)
     up_lin = jnp.dot(expert_rows, expert_up[0], preferred_element_type=jnp.float32)

time: 358 us -> 417 us (1.16)
  waiting for transfers between devices: 186 us -> 252 us
  blocking collectives: 83.5 us -> 58.5 us
  local copies, waits for them, and re-layouts: 15.8 us -> 27.3 us
  starting transfers between devices: 37.3 us -> 45.9 us
    all_to_all x0 -> x2, waiting for transfers between devices: none -> 114 us  [the longest x1 86.8 us: shards(): lax.all_to_all(jnp.stack(tuple((pieces for _ in range(lax.psum(1, 'tp')))...]
    all_gather x1 -> x0, waiting for transfers between devices: 47.7 us -> none  [shards(): arrived = lax.all_gather(pieces, 'tp', axis=2, tiled=True)]
    all_to_all x1 -> x0, blocking collectives: 24.5 us -> none  [sent_to_all(): lax.all_to_all(jnp.broadcast_to(array[None], (size, *array.shape)), axis,...]
    all_to_all x0 -> x2, starting transfers between devices: none -> 8.62 us  [the longest x1 4.86 us: shards(): lax.all_to_all(jnp.stack(tuple((pieces for _ in range(lax.psum(1, 'tp')))...]
    reshape x0 -> x1, local copies, waits for them, and re-layouts: none -> 6.47 us  [shards(): jnp.concatenate(lax.all_to_all(jnp.stack(tuple((pieces for _ in range(lax...]
  transfers between devices with their start and end apart: 7 -> 8, of which waited for: 6 -> 7; matrix products, arithmetic and copies ran while one was open for 4% -> 3% of each run, Pallas kernels for 0% -> 0%
where the time goes in v1:
time: 417 us; the launch traced here: 416 us
  waiting for transfers between devices  252 us (60%)
  blocking collectives  58.5 us (14%)
  starting transfers between devices  45.9 us (11%)
  local copies, waits for them, and re-layouts  27.3 us (7%)
  between operations  13.8 us (3%)
  matrix products  9.56 us (2%)
  other arithmetic  8.26 us (2%)
    all_to_all x1, waiting for transfers between devices, shards(): lax.all_to_all(jnp.stack(tuple((pieces for _ in range(lax.psum(1, 'tp')))...  86.8 us
    all_gather x1, waiting for transfers between devices, sent_together(): lax.all_gather(both, axis, axis=dim, tiled=True)  59.6 us
    all_to_all x2, blocking collectives, moved_by_axis(): lax.all_to_all(blocks, axes[k], split_axis=k, concat_axis=k, tiled=True)  47.4 us
    all_to_all x1, waiting for transfers between devices, shards(): lax.all_to_all(expert_out.reshape(experts, capacity, col_width), SP, spli...  33.1 us
    all_to_all x1, waiting for transfers between devices, sent_to_all(): lax.all_to_all(jnp.broadcast_to(array[None], (size, *array.shape)), axis,...  26.8 us
    ppermute x3, waiting for transfers between devices, passed_along(): lax.ppermute(value, axis, [(source, source + steps) for source in range(l...  26.1 us
    all_to_all x1, waiting for transfers between devices, sent_and_summed(): blocks = lax.all_to_all(split_up(array, dim, size), axis, 0, 0, tiled=True)  19.9 us
    all_to_all x1, starting transfers between devices, shards(): lax.all_to_all(expert_out.reshape(experts, capacity, col_width), SP, spli...  18.2 us
  transfers between devices with their start and end apart: 8, of which 7 were waited for; matrix products, arithmetic and copies ran while one was open for 3% of the time, Pallas kernels for 0%

profile of v1, /device:TPU:65, one launch (start us, length us, event | category | flops | bytes accessed | tf_op | source)
XLA Modules:
  0.0 415.7 jit_solution(1078981677317244205)
XLA Ops:
  7.3 7.1 %collective-permute-start.1 = (bf16[128]{0:T(256)(128)(2,1)S(1)}, bf16[128]{0:T(256)(128)(2,1)S(1)}, u32[]{:S(2)}, u32[]{:S(2)}) collective-permute-start(bf16[128]{0:T(256)(128)(2,1)S(1)} %slice.57), channel_id=1, source_target_pairs={{0,8},{8,16},{16,24},{24,32},{32,40},{40,48},{48,56},{56,64},{64,7... | collective-permute-start | bytes 776 | tf_op jit(solution)/shard_map/ppermute | solution.py:17
  15.1 1.9 collective-permute-start.2
  17.8 6.1 %collective-permute-start = (bf16[128,64]{0,1:T(8,128)(2,1)S(1)}, bf16[128,64]{0,1:T(8,128)(2,1)S(1)}, u32[]{:S(2)}, u32[]{:S(2)}) collective-permute-start(bf16[128,64]{0,1:T(8,128)(2,1)S(1)} %slice.53), channel_id=1, source_target_pairs={{0,8},{8,16},{16,24},{24,32},{32,40},{40,48},{48,56},{56,64},{64,7... | collective-permute-start | bytes 49160 | tf_op jit(solution)/shard_map/ppermute | solution.py:17
  26.4 24.3 %collective-permute-done.1 = bf16[128]{0:T(256)(128)(2,1)S(1)} collective-permute-done((bf16[128]{0:T(256)(128)(2,1)S(1)}, bf16[128]{0:T(256)(128)(2,1)S(1)}, u32[]{:S(2)}, u32[]{:S(2)}) %collective-permute-start.1) | collective-permute-done | bytes 288 | tf_op jit(solution)/shard_map/ppermute | solution.py:17
  50.8 1.9 collective-permute-done.2
  57.9 3.8 all-to-all-start
  64.0 2.4 scatter_custom_fusion
  67.3 19.9 %all-to-all-done = bf16[8,256,256]{2,1,0:T(8,128)(2,1)S(1)} async-done(((bf16[8,256,256]{2,1,0:T(8,128)(2,1)}), bf16[8,256,256]{2,1,0:T(8,128)(2,1)S(1)}, u32[]{:S(2)}, u32[]{:S(2)}) %all-to-all-start) | async-done | bytes 1048608 | tf_op jit(solution)/shard_map/all_to_all | solution.py:28
  88.4 11.1 %psum.7 = f32[256]{0:T(256)S(1)} all-reduce(f32[256]{0:T(256)S(1)} %get-tuple-element.5), channel_id=1, replica_groups=mesh['grp'=2,'sp_0'=16,'sp_1'=2,'tp'=8] {'tp'}, use_global_device_ids=true, to_apply=%region_8.9 | all-reduce | flops 256 | bytes 2048 | tf_op jit(solution)/shard_map/psum | solution.py:150
  99.7 3.9 gather_fusion
  103.8 11.5 %all_to_all.30 = bf16[16,2,1,32,256]{4,3,0,2,1:T(8,128)(2,1)S(1)} all-to-all(bf16[16,2,1,32,256]{4,3,0,2,1:T(8,128)(2,1)S(1)} %copy_select_fusion), channel_id=1, replica_groups=mesh['grp'=2,'sp_0'=16,'sp_1'=2,'tp'=8] {'sp_1'}, dimensions={1} | all-to-all | bytes 1048576 | tf_op jit(solution)/shard_map/all_to_all | solution.py:54
  116.4 3.8 all-to-all-start.4
  120.2 26.8 %all-to-all-done.4 = bf16[8,256,256]{1,2,0:T(8,128)(2,1)S(1)} async-done(((bf16[8,256,256]{1,2,0:T(8,128)(2,1)}), bf16[8,256,256]{1,2,0:T(8,128)(2,1)S(1)}, u32[]{:S(2)}, u32[]{:S(2)}) %all-to-all-start.4) | async-done | bytes 1048608 | tf_op jit(solution)/shard_map/all_to_all | solution.py:34
  147.0 35.9 %all_to_all.31 = bf16[16,2,1,32,256]{4,3,1,2,0:T(8,128)(2,1)S(1)} all-to-all(bf16[16,2,1,32,256]{4,3,1,2,0:T(8,128)(2,1)S(1)} %copy.49), channel_id=1, replica_groups=mesh['grp'=2,'sp_0'=16,'sp_1'=2,'tp'=8] {'sp_0'}, dimensions={0} | all-to-all | bytes 1048576 | tf_op jit(solution)/shard_map/all_to_all | solution.py:54
  182.9 2.5 stack.3
  185.4 4.9 %all-to-all-start.3 = ((bf16[8,32,32,256]{3,2,1,0:T(8,128)(2,1)}), bf16[8,32,32,256]{3,2,1,0:T(8,128)(2,1)}, u32[]{:S(2)}, u32[]{:S(2)}) async-start(bf16[8,32,32,256]{3,2,1,0:T(8,128)(2,1)} %stack.3), calls=%async_computation.3 | async-start | bytes 8388608 | tf_op jit(solution)/shard_map/all_to_all | solution.py:174
  191.5 86.8 %all-to-all-done.3 = bf16[8,32,32,256]{3,2,1,0:T(8,128)(2,1)} async-done(((bf16[8,32,32,256]{3,2,1,0:T(8,128)(2,1)}), bf16[8,32,32,256]{3,2,1,0:T(8,128)(2,1)}, u32[]{:S(2)}, u32[]{:S(2)}) %all-to-all-start.3) | async-done | bytes 4194336 | tf_op jit(solution)/shard_map/all_to_all | solution.py:174
  278.3 6.5 %copy.50 = bf16[32,32,8,256]{3,2,1,0:T(8,128)(2,1)S(1)} copy(bf16[32,32,8,256]{3,1,0,2:T(8,128)(2,1)} %bitcast.18) | data formatting | bytes 8388608 | tf_op jit(solution)/shard_map/reshape | solution.py:173
  289.6 59.6 %all-gather.2.cloned.1.call-done = bf16[1280,1024]{1,0:T(8,128)(2,1)} async-done(((bf16[1280,128]{1,0:T(8,128)(2,1)}), bf16[1280,1024]{1,0:T(8,128)(2,1)}) %all-gather.2.cloned.1.call-update) | async-done | bytes 2621456 | tf_op jit(solution)/shard_map/all_gather | solution.py:70
  349.2 3.1 fusion.2
  352.4 18.2 %all-to-all-start.5 = ((bf16[32,32,256]{2,1,0:T(8,128)(2,1)}), bf16[32,32,256]{2,1,0:T(8,128)(2,1)S(1)}, u32[]{:S(2)}, u32[]{:S(2)}) async-start(bf16[32,32,256]{2,1,0:T(8,128)(2,1)} %bitcast.25), calls=%async_computation.5 | async-start | bytes 1048576 | tf_op jit(solution)/shard_map/all_to_all | solution.py:185
  370.7 33.1 %all-to-all-done.5 = bf16[32,32,256]{2,1,0:T(8,128)(2,1)S(1)} async-done(((bf16[32,32,256]{2,1,0:T(8,128)(2,1)}), bf16[32,32,256]{2,1,0:T(8,128)(2,1)S(1)}, u32[]{:S(2)}, u32[]{:S(2)}) %all-to-all-start.5) | async-done | bytes 524320 | tf_op jit(solution)/shard_map/all_to_all | solution.py:185
  403.9 1.9 gather_fusion.1
  406.8 2.0 fusion.8
  (81 shorter events, 23.0 us)
Async XLA Ops:
  6.5 49.8 %copy-start = (bf16[128,2048]{1,0:T(8,128)(2,1)S(1)}, bf16[128,2048]{1,0:T(8,128)(2,1)}, u32[]{:S(2)}) copy-start(bf16[128,2048]{1,0:T(8,128)(2,1)} %param.24) | copy-start | bytes 1572868
  7.3 43.4 %collective-permute-start.1 = (bf16[128]{0:T(256)(128)(2,1)S(1)}, bf16[128]{0:T(256)(128)(2,1)S(1)}, u32[]{:S(2)}, u32[]{:S(2)}) collective-permute-start(bf16[128]{0:T(256)(128)(2,1)S(1)} %slice.57), channel_id=1, source_target_pairs={{0,8},{8,16},{16,24},{24,32},{32,40},{40,48},{48,56},{56,64},{64,7... | collective-permute-start | bytes 776 | tf_op jit(solution)/shard_map/ppermute | solution.py:17
  15.1 37.6 %collective-permute-start.2 = (bf16[128,64]{0,1:T(8,128)(2,1)S(1)}, bf16[128,64]{0,1:T(8,128)(2,1)S(1)}, u32[]{:S(2)}, u32[]{:S(2)}) collective-permute-start(bf16[128,64]{0,1:T(8,128)(2,1)S(1)} %slice.60), channel_id=1, source_target_pairs={{0,8},{8,16},{16,24},{24,32},{32,40},{40,48},{48,56},{56,64},{64,7... | collective-permute-start | bytes 49160 | tf_op jit(solution)/shard_map/ppermute | solution.py:17
  17.8 37.6 %collective-permute-start = (bf16[128,64]{0,1:T(8,128)(2,1)S(1)}, bf16[128,64]{0,1:T(8,128)(2,1)S(1)}, u32[]{:S(2)}, u32[]{:S(2)}) collective-permute-start(bf16[128,64]{0,1:T(8,128)(2,1)S(1)} %slice.53), channel_id=1, source_target_pairs={{0,8},{8,16},{16,24},{24,32},{32,40},{40,48},{48,56},{56,64},{64,7... | collective-permute-start | bytes 49160 | tf_op jit(solution)/shard_map/ppermute | solution.py:17
  56.1 5.6 %copy-start.4 = (s32[256,2]{0,1:T(2,128)S(1)}, s32[256,2]{0,1:T(2,128)}, u32[]{:S(2)}) copy-start(s32[256,2]{0,1:T(2,128)} %param.21) | copy-start | bytes 6148
  57.9 29.3 %all-to-all-start = ((bf16[8,256,256]{2,1,0:T(8,128)(2,1)}), bf16[8,256,256]{2,1,0:T(8,128)(2,1)S(1)}, u32[]{:S(2)}, u32[]{:S(2)}) async-start(bf16[8,256,256]{2,1,0:T(8,128)(2,1)} %bitcast.109), calls=%async_computation | async-start | bytes 2097152 | tf_op jit(solution)/shard_map/all_to_all | solution.py:28
  116.4 30.6 %all-to-all-start.4 = ((bf16[8,256,256]{1,2,0:T(8,128)(2,1)}), bf16[8,256,256]{1,2,0:T(8,128)(2,1)S(1)}, u32[]{:S(2)}, u32[]{:S(2)}) async-start(bf16[8,256,256]{1,2,0:T(8,128)(2,1)} %broadcast_in_dim.70), calls=%async_computation.4 | async-start | bytes 2097152 | tf_op jit(solution)/shard_map/all_to_all | solution.py:34
  185.4 5.1 %copy-start.3 = (bf16[2048,128]{1,0:T(8,128)(2,1)S(1)}, bf16[2048,128]{1,0:T(8,128)(2,1)}, u32[]{:S(2)}) copy-start(bf16[2048,128]{1,0:T(8,128)(2,1)} %param.29) | copy-start | bytes 1572868
  185.4 5.6 %copy-start.6 = (bf16[2048,128]{1,0:T(8,128)(2,1)S(1)}, bf16[2048,128]{1,0:T(8,128)(2,1)}, u32[]{:S(2)}) copy-start(bf16[2048,128]{1,0:T(8,128)(2,1)} %param.30) | copy-start | bytes 1572868
  185.4 92.9 %all-to-all-start.3 = ((bf16[8,32,32,256]{3,2,1,0:T(8,128)(2,1)}), bf16[8,32,32,256]{3,2,1,0:T(8,128)(2,1)}, u32[]{:S(2)}, u32[]{:S(2)}) async-start(bf16[8,32,32,256]{3,2,1,0:T(8,128)(2,1)} %stack.3), calls=%async_computation.3 | async-start | bytes 8388608 | tf_op jit(solution)/shard_map/all_to_all | solution.py:174
  190.3 159.0 %all-gather.2.cloned.1.call-start = ((), (), s32[]{:S(2)}) async-start(), calls=%async_computation.6 | async-start | bytes 2949120 | tf_op jit(solution)/shard_map/all_gather | solution.py:70
  284.7 1.5 copy-start.1
  286.2 1.3 copy-start.7
  287.5 61.7 %copy-start.8 = (bf16[1,1024,256]{2,1,0:T(8,128)(2,1)S(1)}, bf16[1,1024,256]{2,1,0:T(8,128)(2,1)}, u32[]{:S(2)}) copy-start(bf16[1,1024,256]{2,1,0:T(8,128)(2,1)} %param.28) | copy-start | bytes 1572868
  288.8 81.8 %copy-start.5 = (f32[256,2]{0,1:T(2,128)S(1)}, f32[256,2]{0,1:T(2,128)}, u32[]{:S(2)}) copy-start(f32[256,2]{0,1:T(2,128)} %param.22) | copy-start | bytes 6148
  289.6 117.2 %copy-start.2 = (bf16[1024,256]{1,0:T(8,128)(2,1)S(1)}, bf16[1024,256]{1,0:T(8,128)(2,1)}, u32[]{:S(2)}) copy-start(bf16[1024,256]{1,0:T(8,128)(2,1)} %param.31) | copy-start | bytes 1572868
  352.4 51.5 %all-to-all-start.5 = ((bf16[32,32,256]{2,1,0:T(8,128)(2,1)}), bf16[32,32,256]{2,1,0:T(8,128)(2,1)S(1)}, u32[]{:S(2)}, u32[]{:S(2)}) async-start(bf16[32,32,256]{2,1,0:T(8,128)(2,1)} %bitcast.25), calls=%async_computation.5 | async-start | bytes 1048576 | tf_op jit(solution)/shard_map/all_to_all | solution.py:185
Sparse Core Ops, SparseCore 0:
  289.7 59.4 all-gather.1
